TPU v7x, 32 devices: a whole 2x2x4 slice. The times are simulated.
32 devices in a mesh: sp: 8 (over z, x), tp: 4 (over y, core).
Axes of the slice: x: 2, y: 2, z: 4, core: 2. Of those that a mesh axis runs over, the one named last changes fastest.
Arguments:
- residual: bfloat16 [4096, 2048], P(('sp', 'tp')), may hold values from -6 to 6
- query_small: bfloat16 [4096, 8, 128], P('sp', 'tp'), may hold values from -120 to 120
- key_small: bfloat16 [4096, 8, 128], P('sp', 'tp'), may hold values from -6 to 6
- value_small: bfloat16 [4096, 8, 128], P('sp', 'tp'), may hold values from -6 to 6
- query_large: bfloat16 [4096, 8, 256], P('sp', 'tp'), may hold values from -120 to 120
- key_large: bfloat16 [4096, 8, 256], P('sp', 'tp'), may hold values from -6 to 6
- value_large: bfloat16 [4096, 8, 128], P('sp', 'tp'), may hold values from -6 to 6
- lambda_small: float32 [8], P('tp'), may hold values from 0.3 to 0.8
- lambda_large: float32 [8], P('tp'), may hold values from 0.3 to 0.8
- head_gain: float32 [128], replicated, may hold values from 0.1 to 1.9
- output_small: bfloat16 [1024, 2048], P('tp'), may hold values from -0.125 to 0.125
- output_large: bfloat16 [1024, 2048], P('tp'), may hold values from -0.125 to 0.125
- norm_gain: float32 [2048], replicated, may hold values from 0.1 to 1.9
- gate_weight: bfloat16 [2048, 5632], P('sp', 'tp'), may hold values from -0.125 to 0.125
- up_weight: bfloat16 [2048, 5632], P('sp', 'tp'), may hold values from -0.125 to 0.125
- down_weight: bfloat16 [5632, 2048], P('tp', 'sp'), may hold values from -0.3125 to 0.3125
Outputs:
- block_output: bfloat16 [4096, 2048], P(('sp', 'tp'))
All inputs are finite; a program needn't handle non-finite values.
Results may differ from a plain program's by a relative error of at most 0.015.
Values may be sent and summed in bfloat16 or wider, within the bound.
No kernel may reach another device: no remote copies, remote signals or barrier semaphores. Data moves between devices by JAX's collectives and lax.ppermute only.
A program may use at most 128 MiB of HBM per device.

v0:
```python
import math
import jax
import jax.numpy as jnp
from jax import lax
from jax.sharding import PartitionSpec as P

residual_scale = 8.0**0.25
branch_scale = 0.8
norm_epsilon = 1e-05
masked_score = -1e30


def from_partner(value, axis, distance):
    mask = 2**distance
    pairs = [(source, source ^ mask) for source in range(lax.axis_size(axis))]
    return lax.ppermute(value, axis, pairs)


def layer_norm(values, gains):
    centered = values - jnp.mean(values, axis=-1, keepdims=True)
    variance = jnp.mean(centered * centered, axis=-1, keepdims=True)
    return centered * lax.rsqrt(variance + norm_epsilon) * gains


def empty_state(head_count, tokens, width):
    return (
        jnp.full((head_count, 2, tokens), masked_score, jnp.float32),
        jnp.zeros((head_count, 2, tokens), jnp.float32),
        jnp.zeros((head_count, 2, tokens, width), jnp.float32),
    )


def absorb_group(state, query_maps, key_block, value_block, key_index, query_index):
    running_max, totals, accumulated = state
    head_size = query_maps.shape[3]
    scores = jnp.einsum(
        "qhmd,khmd->hmqk", query_maps, key_block, preferred_element_type=jnp.float32
    ) * head_size ** (-0.5)
    visible = key_index[None, :] <= query_index[:, None]
    scores = jnp.where(visible, scores, masked_score)
    new_max = jnp.maximum(running_max, jnp.max(scores, axis=-1))
    fading = jnp.exp(running_max - new_max)
    weights = jnp.where(visible, jnp.exp(scores - new_max[..., None]), 0.0)
    totals = totals * fading + jnp.sum(weights, axis=-1)
    accumulated = accumulated * fading[..., None] + jnp.einsum(
        "hmqk,khe->hmqe",
        weights.astype(jnp.bfloat16),
        value_block,
        preferred_element_type=jnp.float32,
    )
    return (new_max, totals, accumulated)


def finish_group(state, lambdas, head_gain):
    running_max, totals, accumulated = state
    map_out = accumulated / totals[..., None]
    combined = map_out[:, 0] - lambdas[:, None, None] * map_out[:, 1]
    mean_square = jnp.mean(combined * combined, axis=-1, keepdims=True)
    normed = (combined * lax.rsqrt(mean_square + norm_epsilon) * head_gain * branch_scale).astype(
        jnp.bfloat16
    )
    head_count, tokens, width = normed.shape
    return jnp.transpose(normed, (1, 0, 2)).reshape(tokens, head_count * width)


def per_device(
    residual,
    query_small,
    key_small,
    value_small,
    query_large,
    key_large,
    value_large,
    lambda_small,
    lambda_large,
    head_gain,
    output_small,
    output_large,
    norm_gain,
    gate_weight,
    up_weight,
    down_weight,
):
    tokens = query_small.shape[0]
    half = tokens // 2
    own_rows = residual.shape[0]
    bit_count = lax.axis_size("sp").bit_length() - 1
    residual_all = lax.all_gather(residual, "tp", axis=0, tiled=True)
    heads_small = query_small.shape[1]
    heads_large = query_large.shape[1]
    value_width = value_small.shape[2]
    first_start = lax.axis_index("sp") * tokens
    later_small = query_small[half:]
    later_large = query_large[half:]
    for bit in range(bit_count):
        later_small, later_large = from_partner((later_small, later_large), "sp", bit)
    second_start = (lax.axis_size("sp") - 1 - lax.axis_index("sp")) * tokens + half
    halves = (
        (
            query_small[:half].reshape(half, heads_small, 2, -1),
            query_large[:half].reshape(half, heads_large, 2, -1),
            first_start + jnp.arange(half, dtype=jnp.int32),
        ),
        (
            later_small.reshape(half, heads_small, 2, -1),
            later_large.reshape(half, heads_large, 2, -1),
            second_start + jnp.arange(half, dtype=jnp.int32),
        ),
    )
    one_half = (
        empty_state(heads_small, half, value_width),
        empty_state(heads_large, half, value_width),
    )
    keys_first = lax.all_gather(key_small, "sp", axis=0, tiled=True)
    keys_second = lax.all_gather(key_large, "sp", axis=0, tiled=True)
    values_first = lax.all_gather(value_small, "sp", axis=0, tiled=True)
    values_second = lax.all_gather(value_large, "sp", axis=0, tiled=True)
    row_count = keys_first.shape[0]
    block_size = math.gcd(row_count, 512)
    number = row_count // block_size
    stacked = (
        keys_first.reshape(number, block_size, heads_small, 2, -1),
        keys_second.reshape(number, block_size, heads_large, 2, -1),
        values_first.reshape(number, block_size, heads_small, value_width),
        values_second.reshape(number, block_size, heads_large, value_width),
    )

    def step(carried, block_items):
        block_index, blocks = block_items
        key_index = block_index * block_size + jnp.arange(block_size, dtype=jnp.int32)
        updated = []
        for which in range(2):
            maps_small, maps_large, query_index = halves[which]

            def take(pair):
                return (
                    absorb_group(pair[0], maps_small, blocks[0], blocks[2], key_index, query_index),
                    absorb_group(pair[1], maps_large, blocks[1], blocks[3], key_index, query_index),
                )

            def leave(pair):
                return pair

            updated.append(
                lax.cond(key_index[0] <= query_index[half - 1], take, leave, carried[which])
            )
        return ((updated[0], updated[1]), None)

    result, unused = lax.scan(
        step, (one_half, one_half), (jnp.arange(number, dtype=jnp.int32), stacked)
    )
    first_states, second_states = result
    early_small = finish_group(first_states[0], lambda_small, head_gain)
    early_large = finish_group(first_states[1], lambda_large, head_gain)
    late_small = finish_group(second_states[0], lambda_small, head_gain)
    late_large = finish_group(second_states[1], lambda_large, head_gain)
    for bit in range(bit_count):
        late_small, late_large = from_partner((late_small, late_large), "sp", bit)
    attended_small = jnp.concatenate([early_small, late_small], axis=0)
    attended_large = jnp.concatenate([early_large, late_large], axis=0)
    mixed_sum = lax.psum(
        (
            jnp.dot(attended_small, output_small, preferred_element_type=jnp.float32)
            + jnp.dot(attended_large, output_large, preferred_element_type=jnp.float32)
        ).astype(jnp.bfloat16),
        "tp",
    ).astype(jnp.float32)
    whole_rows = layer_norm(
        residual_scale * residual_all.astype(jnp.float32) + mixed_sum, norm_gain
    ).astype(jnp.bfloat16)
    normed = lax.dynamic_slice_in_dim(whole_rows, lax.axis_index("tp") * own_rows, own_rows, 0)
    gate_rows = jnp.dot(
        whole_rows,
        lax.all_gather(gate_weight, "sp", axis=0, tiled=True),
        preferred_element_type=jnp.float32,
    )
    up_rows = jnp.dot(
        whole_rows,
        lax.all_gather(up_weight, "sp", axis=0, tiled=True),
        preferred_element_type=jnp.float32,
    )
    down_full = lax.all_gather(down_weight, "sp", axis=1, tiled=True)
    hidden = (jax.nn.silu(gate_rows) * up_rows).astype(jnp.bfloat16)
    down_sum = lax.psum_scatter(
        jnp.dot(hidden, down_full, preferred_element_type=jnp.float32).astype(jnp.bfloat16),
        "tp",
        scatter_dimension=0,
        tiled=True,
    ).astype(jnp.float32)
    return (residual_scale * normed.astype(jnp.float32) + 0.5 * down_sum).astype(jnp.bfloat16)


def solution(mesh):
    in_specs = (
        P(("sp", "tp"), None),
        P("sp", "tp", None),
        P("sp", "tp", None),
        P("sp", "tp", None),
        P("sp", "tp", None),
        P("sp", "tp", None),
        P("sp", "tp", None),
        P("tp"),
        P("tp"),
        P(),
        P("tp", None),
        P("tp", None),
        P(),
        P("sp", "tp"),
        P("sp", "tp"),
        P("tp", "sp"),
    )
    out_specs = P(("sp", "tp"), None)
    return jax.shard_map(
        per_device, mesh=mesh, in_specs=in_specs, out_specs=out_specs, check_vma=False
    )
```

profile of v0, /device:TPU:0, one launch (start us, length us, event | category | flops | bytes accessed | tf_op | source)
XLA Modules:
  0.0 791.7 jit_solution(11565010698791997182)
XLA Ops:
  15.2 6.3 collective-permute-done.3
  30.0 7.0 collective-permute-done.4
  43.6 29.2 %collective-permute-done.2 = bf16[256,2,128]{2,1,0:T(2,128)(2,1)S(1)} collective-permute-done((bf16[256,2,128]{2,1,0:T(2,128)(2,1)S(1)}, bf16[256,2,128]{2,1,0:T(2,128)(2,1)S(1)}, u32[]{:S(2)}, u32[]{:S(2)}) %collective-permute-start.2) | collective-permute-done | bytes 131104 | tf_op jit(solution)/shard_map/ppermute | solution.py:16
  73.8 9.7 %reshape.126 = bf16[8,512,2,2,64]{4,3,2,1,0:T(2,128)(2,1)} reshape(bf16[4096,2,128]{2,1,0:T(2,128)(2,1)} %all-gather.11.cloned.1.call-done) | data formatting | bytes 4194304 | tf_op jit(solution)/shard_map/reshape | solution.py:122
  83.5 10.6 %copy.56 = bf16[8,512,2,2,64]{1,4,3,2,0:T(8,128)(2,1)} copy(bf16[8,512,2,2,64]{4,3,2,1,0:T(2,128)(2,1)} %reshape.126) | data formatting | bytes 4194304 | tf_op jit(solution)/shard_map/while | solution.py:149
  94.1 54.6 %all-gather.15.cloned.1.call-done = bf16[4096,2,256]{2,1,0:T(2,128)(2,1)} async-done(((bf16[512,2,256]{2,1,0:T(2,128)(2,1)}), bf16[4096,2,256]{2,1,0:T(2,128)(2,1)}) %all-gather.15.cloned.1.call-update) | async-done | bytes 4194320 | tf_op jit(solution)/shard_map/all_gather | solution.py:115
  148.7 11.7 %reshape.127 = bf16[8,512,2,2,128]{4,3,2,1,0:T(2,128)(2,1)} reshape(bf16[4096,2,256]{2,1,0:T(2,128)(2,1)} %all-gather.15.cloned.1.call-done) | data formatting | bytes 8388608 | tf_op jit(solution)/shard_map/reshape | solution.py:123
  160.4 38.1 %all-gather.13.cloned.1.call-done = bf16[4096,2,128]{2,0,1:T(8,128)(2,1)} async-done(((bf16[512,2,128]{2,0,1:T(8,128)(2,1)}), bf16[4096,2,128]{2,0,1:T(8,128)(2,1)}) %all-gather.13.cloned.1.call-update) | async-done | bytes 2097168 | tf_op jit(solution)/shard_map/all_gather | solution.py:116
  198.5 49.7 %all-gather.17.cloned.1.call-done = bf16[4096,2,128]{2,0,1:T(8,128)(2,1)} async-done(((bf16[512,2,128]{2,0,1:T(8,128)(2,1)}), bf16[4096,2,128]{2,0,1:T(8,128)(2,1)}) %all-gather.17.cloned.1.call-update) | async-done | bytes 2097168 | tf_op jit(solution)/shard_map/all_gather | solution.py:117
  251.6 124.7 %while.32 = (s32[]{:T(128)}, f32[2,2,256]{2,1,0:T(2,128)S(1)}, f32[2,2,256]{2,1,0:T(2,128)S(1)}, f32[2,2,256,128]{3,2,1,0:T(8,128)}, f32[2,2,256]{2,1,0:T(2,128)...) while((s32[]{:T(128)}, f32[2,2,256]{2,1,0:T(2,128)S(1)}, ...), condition=%wide.region_13.14_spmd, body=%wide.region_0.13_spmd.sunk | while | flops 968106496 | bytes 58991568 | solution.py:149
  258.8 5.7 conditional.5
  266.5 5.8 conditional.4
  279.4 5.7 conditional.5
  309.1 5.7 conditional.5
  323.9 5.7 conditional.5
  338.8 5.7 conditional.5
  353.6 5.7 conditional.5
  410.6 48.7 %all-reduce.2.cloned.1.call-done = bf16[512,2048]{1,0:T(8,128)(2,1)} async-done(((bf16[512,2048]{1,0:T(8,128)(2,1)}), bf16[512,2048]{1,0:T(8,128)(2,1)}) %all-reduce.2.cloned.1.call-update) | async-done | bytes 2097168 | tf_op jit(solution)/shard_map/psum | solution.py:161
  465.9 88.0 %all-gather.19.cloned.1.call-done = bf16[2048,1408]{1,0:T(8,128)(2,1)} async-done(((bf16[256,1408]{1,0:T(8,128)(2,1)}), bf16[2048,1408]{1,0:T(8,128)(2,1)}) %all-gather.19.cloned.1.call-update) | async-done | bytes 5767184 | tf_op jit(solution)/shard_map/all_gather | solution.py:174
  553.9 8.2 %fusion.72 = f32[512,1408]{1,0:T(8,128)} fusion(bf16[512,2048]{1,0:T(8,128)(2,1)} %multiply_convert_fusion, bf16[2048,1408]{1,0:T(8,128)(2,1)} %all-gather.19.cloned.1.call-done), kind=kOutput, calls=%fused_computation.131 | convolution fusion | flops 2952790016 | bytes 10747904 | tf_op jit(solution)/shard_map/dot_general | solution.py:172
  562.1 84.5 %all-gather.21.cloned.1.call-done = bf16[2048,1408]{1,0:T(8,128)(2,1)} async-done(((bf16[256,1408]{1,0:T(8,128)(2,1)}), bf16[2048,1408]{1,0:T(8,128)(2,1)}) %all-gather.21.cloned.1.call-update) | async-done | bytes 5767184 | tf_op jit(solution)/shard_map/all_gather | solution.py:179
  646.6 93.4 %all-gather.23.cloned.1.call-done = bf16[1408,2048]{1,0:T(8,128)(2,1)} async-done(((bf16[1408,256]{1,0:T(8,128)(2,1)}), bf16[1408,2048]{1,0:T(8,128)(2,1)}) %all-gather.23.cloned.1.call-update) | async-done | bytes 5767184 | tf_op jit(solution)/shard_map/all_gather | solution.py:182
  740.0 13.3 %convolution_convert_fusion = bf16[512,2048]{1,0:T(8,128)(2,1)} fusion(bf16[1408,2048]{1,0:T(8,128)(2,1)} %all-gather.23.cloned.1.call-done, bf16[512,2048]{1,0:T(8,128)(2,1)S(1)} %copy-done.3, bf16[2048,1408]{1,0:T(8,128)(2,1)} %all-gather.21.cloned.1.call-done, f32[512,1408]{1,0:T(8,128)} %fusion.72), kind=kOutput, calls=%fused_computation.79 | convolution fusion | flops 5910953984 | bytes 18612224 | tf_op jit(solution)/shard_map/dot_general | solution.py:185
  753.3 29.5 %reduce-scatter.2.cloned.1.call-done = bf16[128,2048]{1,0:T(8,128)(2,1)} async-done(((bf16[512,2048]{1,0:T(8,128)(2,1)}), bf16[128,2048]{1,0:T(8,128)(2,1)}) %reduce-scatter.2.cloned.1.call-update) | async-done | bytes 524304 | tf_op jit(solution)/shard_map/reduce_scatter | solution.py:184
  (376 shorter events, 180.5 us)
Async XLA Ops:
  6.5 396.8 %copy-start = (bf16[256,2048]{1,0:T(8,128)(2,1)S(1)}, bf16[256,2048]{1,0:T(8,128)(2,1)}, u32[]{:S(2)}) copy-start(bf16[256,2048]{1,0:T(8,128)(2,1)} %param.33) | copy-start | bytes 3145732
  6.5 67.3 %all-gather.11.cloned.1.call-start = ((), (), s32[]{:S(2)}) async-start(), calls=%async_computation.2 | async-start | bytes 2359296 | tf_op jit(solution)/shard_map/all_gather | solution.py:114
  7.3 141.4 %all-gather.15.cloned.1.call-start = ((), (), s32[]{:S(2)}) async-start(), calls=%async_computation.4 | async-start | bytes 4718592 | tf_op jit(solution)/shard_map/all_gather | solution.py:115
  8.0 190.5 %all-gather.13.cloned.1.call-start = ((), (), s32[]{:S(2)}) async-start(), calls=%async_computation.3 | async-start | bytes 2359296 | tf_op jit(solution)/shard_map/all_gather | solution.py:116
  9.8 238.4 %all-gather.17.cloned.1.call-start = ((), (), s32[]{:S(2)}) async-start(), calls=%async_computation.5 | async-start | bytes 2359296 | tf_op jit(solution)/shard_map/all_gather | solution.py:117
  11.5 399.0 %all-gather.9.cloned.1.call-start = ((), (), s32[]{:S(2)}) async-start(), calls=%async_computation.1 | async-start | bytes 2621440 | tf_op jit(solution)/shard_map/all_gather | solution.py:88
  12.2 9.3 %collective-permute-start.3 = (bf16[256,2,256]{0,2,1:T(8,128)(2,1)S(1)}, bf16[256,2,256]{0,2,1:T(8,128)(2,1)S(1)}, u32[]{:S(2)}, u32[]{:S(2)}) collective-permute-start(bf16[256,2,256]{0,2,1:T(8,128)(2,1)S(1)} %copy.82), channel_id=1, source_target_pairs={{0,4},{4,0},{8,12},{12,8},{16,20},{20,16},{24,28},{28,24},{1,5},{5... | collective-permute-start | bytes 786440 | tf_op jit(solution)/shard_map/ppermute | solution.py:16
  21.5 15.5 %collective-permute-start.4 = (bf16[256,2,256]{0,2,1:T(8,128)(2,1)S(1)}, bf16[256,2,256]{0,2,1:T(8,128)(2,1)S(1)}, u32[]{:S(2)}, u32[]{:S(2)}) collective-permute-start(bf16[256,2,256]{0,2,1:T(8,128)(2,1)S(1)} %collective-permute-done.3), channel_id=1, source_target_pairs={{0,8},{4,12},{8,0},{12,4},{16,24},{20,28},{24,16},{28,20},{1,9},{5... | collective-permute-start | bytes 786440 | tf_op jit(solution)/shard_map/ppermute | solution.py:16
  23.5 5.0 collective-permute-start
  28.5 12.9 %collective-permute-start.1 = (bf16[256,2,128]{2,1,0:T(2,128)(2,1)S(1)}, bf16[256,2,128]{2,1,0:T(2,128)(2,1)S(1)}, u32[]{:S(2)}, u32[]{:S(2)}) collective-permute-start(bf16[256,2,128]{2,1,0:T(2,128)(2,1)S(1)} %collective-permute-done), channel_id=1, source_target_pairs={{0,8},{4,12},{8,0},{12,4},{16,24},{20,28},{24,16},{28,20},{1,9},{5... | collective-permute-start | bytes 393224 | tf_op jit(solution)/shard_map/ppermute | solution.py:16
  37.0 35.9 %collective-permute-start.5 = (bf16[256,2,256]{0,2,1:T(8,128)(2,1)S(1)}, bf16[256,2,256]{0,2,1:T(8,128)(2,1)S(1)}, u32[]{:S(2)}, u32[]{:S(2)}) collective-permute-start(bf16[256,2,256]{0,2,1:T(8,128)(2,1)S(1)} %collective-permute-done.4), channel_id=1, source_target_pairs={{0,16},{4,20},{8,24},{12,28},{16,0},{20,4},{24,8},{28,12},{1,17},{... | collective-permute-start | bytes 786440 | tf_op jit(solution)/shard_map/ppermute | solution.py:16
  41.5 31.3 %collective-permute-start.2 = (bf16[256,2,128]{2,1,0:T(2,128)(2,1)S(1)}, bf16[256,2,128]{2,1,0:T(2,128)(2,1)S(1)}, u32[]{:S(2)}, u32[]{:S(2)}) collective-permute-start(bf16[256,2,128]{2,1,0:T(2,128)(2,1)S(1)} %collective-permute-done.1), channel_id=1, source_target_pairs={{0,16},{4,20},{8,24},{12,28},{16,0},{20,4},{24,8},{28,12},{1,17},{... | collective-permute-start | bytes 393224 | tf_op jit(solution)/shard_map/ppermute | solution.py:16
  43.0 416.3 %all-reduce.2.cloned.1.call-start = ((), (), s32[]{:S(2)}) async-start(), calls=%async_computation.6 | async-start | bytes 4194304 | tf_op jit(solution)/shard_map/psum | solution.py:161
  384.5 5.0 collective-permute-start.9
  385.1 6.5 collective-permute-start.6
  389.6 5.1 collective-permute-start.10
  391.6 6.7 collective-permute-start.7
  394.7 8.6 %collective-permute-start.11 = (bf16[256,256]{0,1:T(8,128)(2,1)S(1)}, bf16[256,256]{0,1:T(8,128)(2,1)S(1)}, u32[]{:S(2)}, u32[]{:S(2)}) collective-permute-start(bf16[256,256]{0,1:T(8,128)(2,1)S(1)} %collective-permute-done.10), channel_id=1, source_target_pairs={{0,16},{4,20},{8,24},{12,28},{16,0},{20,4},{24,8},{28,12},{1,17},{... | collective-permute-start | bytes 393224 | tf_op jit(solution)/shard_map/ppermute | solution.py:16
  398.3 7.9 collective-permute-start.8
  408.3 145.6 %all-gather.19.cloned.1.call-start = ((), (), s32[]{:S(2)}) async-start(), calls=%async_computation.7 | async-start | bytes 6488064 | tf_op jit(solution)/shard_map/all_gather | solution.py:174
  409.0 237.6 %all-gather.21.cloned.1.call-start = ((), (), s32[]{:S(2)}) async-start(), calls=%async_computation.8 | async-start | bytes 6488064 | tf_op jit(solution)/shard_map/all_gather | solution.py:179
  409.8 330.2 %all-gather.23.cloned.1.call-start = ((), (), s32[]{:S(2)}) async-start(), calls=%async_computation.9 | async-start | bytes 6488064 | tf_op jit(solution)/shard_map/all_gather | solution.py:182
  410.5 372.3 %reduce-scatter.2.cloned.1.call-start = ((), (), s32[]{:S(2)}) async-start(), calls=%async_computation.10 | async-start | bytes 2621440 | tf_op jit(solution)/shard_map/reduce_scatter | solution.py:184
  465.9 274.1 %copy-start.3 = (bf16[512,2048]{1,0:T(8,128)(2,1)S(1)}, bf16[512,2048]{1,0:T(8,128)(2,1)}, u32[]{:S(2)}) copy-start(bf16[512,2048]{1,0:T(8,128)(2,1)} %multiply_convert_fusion) | copy-start | bytes 6291460
  (49 other events, 137.6 us)
Sparse Core Ops, SparseCore 0:
  9.5 64.2 all-gather.10
  75.9 72.7 all-gather.14
  150.9 47.5 all-gather.12
  200.6 47.5 all-gather.16
  249.6 21.0 all-gather.8
  408.4 50.8 all-reduce.1
  461.5 92.3 all-gather.18
  556.1 90.4 all-gather.20
  648.7 91.2 all-gather.22
  753.4 29.3 reduce-scatter.1
where the time goes:
time: 794 us; the launch traced here: 792 us
  waiting for transfers between devices  548 us (69%)
  local copies, waits for them, and re-layouts  102 us (13%)
  matrix products  52.3 us (7%)
  loops' own time  26.4 us (3%)
  other arithmetic  25.5 us (3%)
  starting transfers between devices  23.7 us (3%)
  between operations  13.9 us (2%)
    all_gather x1, waiting for transfers between devices, per_device(): down_full = lax.all_gather(down_weight, 'sp', axis=1, tiled=True)  93.4 us
    all_gather x1, waiting for transfers between devices, per_device(): lax.all_gather(gate_weight, 'sp', axis=0, tiled=True)  88 us
    all_gather x1, waiting for transfers between devices, per_device(): lax.all_gather(up_weight, 'sp', axis=0, tiled=True)  84.5 us
    ppermute x12, waiting for transfers between devices, from_partner(): return lax.ppermute(value, axis, pairs)  57.4 us
    all_gather x1, waiting for transfers between devices, per_device(): keys_second = lax.all_gather(key_large, 'sp', axis=0, tiled=True)  54.6 us
    all_gather x1, waiting for transfers between devices, per_device(): values_second = lax.all_gather(value_large, 'sp', axis=0, tiled=True)  49.7 us
    psum x1, waiting for transfers between devices, per_device(): lax.psum((jnp.dot(attended_small, output_small, preferred_element_type=jn...  48.7 us
    all_gather x1, waiting for transfers between devices, per_device(): values_first = lax.all_gather(value_small, 'sp', axis=0, tiled=True)  38.1 us
  transfers between devices with their start and end apart: 22, of which 18 were waited for; matrix products, arithmetic and copies ran while one was open for 20% of the time, Pallas kernels for 0%

commit v1 on v0

--- a/solution.py
+++ b/solution.py
@@ -114,7 +114,14 @@
     keys_first = lax.all_gather(key_small, "sp", axis=0, tiled=True)
     keys_second = lax.all_gather(key_large, "sp", axis=0, tiled=True)
     values_first = lax.all_gather(value_small, "sp", axis=0, tiled=True)
-    values_second = lax.all_gather(value_large, "sp", axis=0, tiled=True)
+    pages = [value_large]
+    n = lax.axis_size("sp")
+    for src_i in range(n - 1):
+        answer = lax.ppermute(pages[-1], "sp", [(k0, (k0 + 1) % n) for k0 in range(n)])
+        pages.append(answer)
+    state_now = jnp.concatenate(pages[::-1], 0)
+    val2 = lax.axis_index("sp")
+    values_second = jnp.roll(state_now, (val2 + 1) * value_large.shape[0], 0)
     row_count = keys_first.shape[0]
     block_size = math.gcd(row_count, 512)
     number = row_count // block_size

time: 794 us -> 769 us (0.969)
  waiting for transfers between devices: 548 us -> 520 us
  local copies, waits for them, and re-layouts: 102 us -> 110 us
    ppermute x0 -> x7, waiting for transfers between devices: none -> 57.8 us  [per_device(): lax.ppermute(pages[-1], 'sp', [(k0, (k0 + 1) % n) for k0 in range(n)])]
    all_gather x1 -> x0, waiting for transfers between devices: 49.7 us -> none  [per_device(): values_second = lax.all_gather(value_large, 'sp', axis=0, tiled=True)]
    all_gather x1, waiting for transfers between devices: 54.6 us -> 28.9 us  [per_device(): keys_second = lax.all_gather(key_large, 'sp', axis=0, tiled=True)]
    ppermute x12, starting transfers between devices: 23.3 us -> 14.2 us  [from_partner(): return lax.ppermute(value, axis, pairs)]
    ppermute x12, waiting for transfers between devices: 57.4 us -> 48.5 us  [from_partner(): return lax.ppermute(value, axis, pairs)]
  transfers between devices with their start and end apart: 22 -> 28, of which waited for: 18 -> 22; matrix products, arithmetic and copies ran while one was open for 20% -> 21% of each run, Pallas kernels for 0% -> 0%
where the time goes in v1:
time: 769 us; the launch traced here: 766 us
  waiting for transfers between devices  520 us (68%)
  local copies, waits for them, and re-layouts  110 us (14%)
  matrix products  52.3 us (7%)
  loops' own time  27 us (4%)
  other arithmetic  25.5 us (3%)
  starting transfers between devices  17.6 us (2%)
  between operations  13.7 us (2%)
    all_gather x1, waiting for transfers between devices, per_device(): down_full = lax.all_gather(down_weight, 'sp', axis=1, tiled=True)  93.4 us
    all_gather x1, waiting for transfers between devices, per_device(): lax.all_gather(gate_weight, 'sp', axis=0, tiled=True)  87.9 us
    all_gather x1, waiting for transfers between devices, per_device(): lax.all_gather(up_weight, 'sp', axis=0, tiled=True)  84.5 us
    ppermute x7, waiting for transfers between devices, per_device(): lax.ppermute(pages[-1], 'sp', [(k0, (k0 + 1) % n) for k0 in range(n)])  57.8 us
    ppermute x12, waiting for transfers between devices, from_partner(): return lax.ppermute(value, axis, pairs)  48.5 us
    psum x1, waiting for transfers between devices, per_device(): lax.psum((jnp.dot(attended_small, output_small, preferred_element_type=jn...  48.5 us
    all_gather x1, waiting for transfers between devices, per_device(): values_first = lax.all_gather(value_small, 'sp', axis=0, tiled=True)  38.1 us
    reduce_scatter x1, waiting for transfers between devices, per_device(): lax.psum_scatter(jnp.dot(hidden, down_full, preferred_element_type=jnp.fl...  29.5 us
  transfers between devices with their start and end apart: 28, of which 22 were waited for; matrix products, arithmetic and copies ran while one was open for 21% of the time, Pallas kernels for 0%

profile of v1, /device:TPU:0, one launch (start us, length us, event | category | flops | bytes accessed | tf_op | source)
XLA Modules:
  0.0 766.2 jit_solution(10103897854299725620)
XLA Ops:
  13.8 9.4 %collective-permute-done = bf16[512,2,128]{2,0,1:T(8,128)(2,1)S(1)} collective-permute-done((bf16[512,2,128]{2,0,1:T(8,128)(2,1)S(1)}, bf16[512,2,128]{2,0,1:T(8,128)(2,1)S(1)}, u32[]{:S(2)}, u32[]{:S(2)}) %collective-permute-start) | collective-permute-done | bytes 262176 | tf_op jit(solution)/shard_map/ppermute | solution.py:120
  23.2 16.6 %collective-permute-done.1 = bf16[512,2,128]{2,0,1:T(8,128)(2,1)S(1)} collective-permute-done((bf16[512,2,128]{2,0,1:T(8,128)(2,1)S(1)}, bf16[512,2,128]{2,0,1:T(8,128)(2,1)S(1)}, u32[]{:S(2)}, u32[]{:S(2)}) %collective-permute-start.1) | collective-permute-done | bytes 262176 | tf_op jit(solution)/shard_map/ppermute | solution.py:120
  39.8 14.0 %collective-permute-done.2 = bf16[512,2,128]{2,0,1:T(8,128)(2,1)S(1)} collective-permute-done((bf16[512,2,128]{2,0,1:T(8,128)(2,1)S(1)}, bf16[512,2,128]{2,0,1:T(8,128)(2,1)S(1)}, u32[]{:S(2)}, u32[]{:S(2)}) %collective-permute-start.2) | collective-permute-done | bytes 262176 | tf_op jit(solution)/shard_map/ppermute | solution.py:120
  54.4 12.1 %collective-permute-done.3 = bf16[512,2,128]{2,0,1:T(8,128)(2,1)S(1)} collective-permute-done((bf16[512,2,128]{2,0,1:T(8,128)(2,1)S(1)}, bf16[512,2,128]{2,0,1:T(8,128)(2,1)S(1)}, u32[]{:S(2)}, u32[]{:S(2)}) %collective-permute-start.3) | collective-permute-done | bytes 262176 | tf_op jit(solution)/shard_map/ppermute | solution.py:120
  66.5 8.6 %collective-permute-done.10 = bf16[256,2,256]{0,2,1:T(8,128)(2,1)S(1)} collective-permute-done((bf16[256,2,256]{0,2,1:T(8,128)(2,1)S(1)}, bf16[256,2,256]{0,2,1:T(8,128)(2,1)S(1)}, u32[]{:S(2)}, u32[]{:S(2)}) %collective-permute-start.10) | collective-permute-done | bytes 262176 | tf_op jit(solution)/shard_map/ppermute | solution.py:16
  80.1 7.4 collective-permute-done.7
  95.6 19.1 %collective-permute-done.9 = bf16[256,2,128]{2,1,0:T(2,128)(2,1)S(1)} collective-permute-done((bf16[256,2,128]{2,1,0:T(2,128)(2,1)S(1)}, bf16[256,2,128]{2,1,0:T(2,128)(2,1)S(1)}, u32[]{:S(2)}, u32[]{:S(2)}) %collective-permute-start.9) | collective-permute-done | bytes 131104 | tf_op jit(solution)/shard_map/ppermute | solution.py:16
  122.8 9.7 %reshape.126 = bf16[8,512,2,2,64]{4,3,2,1,0:T(2,128)(2,1)} reshape(bf16[4096,2,128]{2,1,0:T(2,128)(2,1)} %all-gather.10.cloned.1.call-done) | data formatting | bytes 4194304 | tf_op jit(solution)/shard_map/reshape | solution.py:129
  132.5 10.7 %copy.60 = bf16[8,512,2,2,64]{1,4,3,2,0:T(8,128)(2,1)} copy(bf16[8,512,2,2,64]{4,3,2,1,0:T(2,128)(2,1)} %reshape.126) | data formatting | bytes 4194304 | tf_op jit(solution)/shard_map/while | solution.py:156
  143.1 28.9 %all-gather.14.cloned.1.call-done = bf16[4096,2,256]{2,1,0:T(2,128)(2,1)} async-done(((bf16[512,2,256]{2,1,0:T(2,128)(2,1)}), bf16[4096,2,256]{2,1,0:T(2,128)(2,1)}) %all-gather.14.cloned.1.call-update) | async-done | bytes 4194320 | tf_op jit(solution)/shard_map/all_gather | solution.py:115
  172.0 11.7 %reshape.127 = bf16[8,512,2,2,128]{4,3,2,1,0:T(2,128)(2,1)} reshape(bf16[4096,2,256]{2,1,0:T(2,128)(2,1)} %all-gather.14.cloned.1.call-done) | data formatting | bytes 8388608 | tf_op jit(solution)/shard_map/reshape | solution.py:130
  183.7 38.1 %all-gather.12.cloned.1.call-done = bf16[4096,2,128]{2,0,1:T(8,128)(2,1)} async-done(((bf16[512,2,128]{2,0,1:T(8,128)(2,1)}), bf16[4096,2,128]{2,0,1:T(8,128)(2,1)}) %all-gather.12.cloned.1.call-update) | async-done | bytes 2097168 | tf_op jit(solution)/shard_map/all_gather | solution.py:116
  225.2 126.4 %while.32 = (s32[]{:T(128)}, f32[2,2,256]{2,1,0:T(2,128)S(1)}, f32[2,2,256]{2,1,0:T(2,128)S(1)}, f32[2,2,256,128]{3,2,1,0:T(8,128)}, f32[2,2,256]{2,1,0:T(2,128)...) while((s32[]{:T(128)}, f32[2,2,256]{2,1,0:T(2,128)S(1)}, ...), condition=%wide.region_13.14_spmd, body=%wide.region_0.13_spmd.sunk | while | flops 968106496 | bytes 58991568 | solution.py:156
  232.7 5.8 conditional.5
  253.4 5.8 conditional.5
  268.5 5.8 conditional.5
  283.5 5.8 conditional.5
  385.9 48.5 %all-reduce.2.cloned.1.call-done = bf16[512,2048]{1,0:T(8,128)(2,1)} async-done(((bf16[512,2048]{1,0:T(8,128)(2,1)}), bf16[512,2048]{1,0:T(8,128)(2,1)}) %all-reduce.2.cloned.1.call-update) | async-done | bytes 2097168 | tf_op jit(solution)/shard_map/psum | solution.py:168
  440.9 87.9 %all-gather.16.cloned.1.call-done = bf16[2048,1408]{1,0:T(8,128)(2,1)} async-done(((bf16[256,1408]{1,0:T(8,128)(2,1)}), bf16[2048,1408]{1,0:T(8,128)(2,1)}) %all-gather.16.cloned.1.call-update) | async-done | bytes 5767184 | tf_op jit(solution)/shard_map/all_gather | solution.py:181
  528.8 8.2 %fusion.72 = f32[512,1408]{1,0:T(8,128)} fusion(bf16[512,2048]{1,0:T(8,128)(2,1)} %multiply_convert_fusion, bf16[2048,1408]{1,0:T(8,128)(2,1)} %all-gather.16.cloned.1.call-done), kind=kOutput, calls=%fused_computation.148 | convolution fusion | flops 2952790016 | bytes 10747904 | tf_op jit(solution)/shard_map/dot_general | solution.py:179
  537.0 84.5 %all-gather.18.cloned.1.call-done = bf16[2048,1408]{1,0:T(8,128)(2,1)} async-done(((bf16[256,1408]{1,0:T(8,128)(2,1)}), bf16[2048,1408]{1,0:T(8,128)(2,1)}) %all-gather.18.cloned.1.call-update) | async-done | bytes 5767184 | tf_op jit(solution)/shard_map/all_gather | solution.py:186
  621.5 93.4 %all-gather.20.cloned.1.call-done = bf16[1408,2048]{1,0:T(8,128)(2,1)} async-done(((bf16[1408,256]{1,0:T(8,128)(2,1)}), bf16[1408,2048]{1,0:T(8,128)(2,1)}) %all-gather.20.cloned.1.call-update) | async-done | bytes 5767184 | tf_op jit(solution)/shard_map/all_gather | solution.py:189
  714.9 13.2 %convolution_convert_fusion = bf16[512,2048]{1,0:T(8,128)(2,1)} fusion(bf16[1408,2048]{1,0:T(8,128)(2,1)} %all-gather.20.cloned.1.call-done, bf16[512,2048]{1,0:T(8,128)(2,1)S(1)} %copy-done.3, bf16[2048,1408]{1,0:T(8,128)(2,1)} %all-gather.18.cloned.1.call-done, f32[512,1408]{1,0:T(8,128)} %fusion.72), kind=kOutput, calls=%fused_computation.79 | convolution fusion | flops 5910953984 | bytes 18612224 | tf_op jit(solution)/shard_map/dot_general | solution.py:192
  728.1 29.5 %reduce-scatter.2.cloned.1.call-done = bf16[128,2048]{1,0:T(8,128)(2,1)} async-done(((bf16[512,2048]{1,0:T(8,128)(2,1)}), bf16[128,2048]{1,0:T(8,128)(2,1)}) %reduce-scatter.2.cloned.1.call-update) | async-done | bytes 524304 | tf_op jit(solution)/shard_map/reduce_scatter | solution.py:191
  (408 shorter events, 203.2 us)
Async XLA Ops:
  6.5 116.3 %all-gather.10.cloned.1.call-start = ((), (), s32[]{:S(2)}) async-start(), calls=%async_computation.2 | async-start | bytes 2359296 | tf_op jit(solution)/shard_map/all_gather | solution.py:114
  7.3 164.7 %all-gather.14.cloned.1.call-start = ((), (), s32[]{:S(2)}) async-start(), calls=%async_computation.4 | async-start | bytes 4718592 | tf_op jit(solution)/shard_map/all_gather | solution.py:115
  8.0 213.8 %all-gather.12.cloned.1.call-start = ((), (), s32[]{:S(2)}) async-start(), calls=%async_computation.3 | async-start | bytes 2359296 | tf_op jit(solution)/shard_map/all_gather | solution.py:116
  9.8 376.1 %all-gather.8.cloned.1.call-start = ((), (), s32[]{:S(2)}) async-start(), calls=%async_computation.1 | async-start | bytes 2621440 | tf_op jit(solution)/shard_map/all_gather | solution.py:88
  10.8 12.4 %collective-permute-start = (bf16[512,2,128]{2,0,1:T(8,128)(2,1)S(1)}, bf16[512,2,128]{2,0,1:T(8,128)(2,1)S(1)}, u32[]{:S(2)}, u32[]{:S(2)}) collective-permute-start(bf16[512,2,128]{2,0,1:T(8,128)(2,1)S(1)} %copy.53), channel_id=1, source_target_pairs={{0,4},{4,8},{8,12},{12,16},{16,20},{20,24},{24,28},{28,0},{1,5},{5... | collective-permute-start | bytes 786440 | tf_op jit(solution)/shard_map/ppermute | solution.py:120
  23.2 16.6 %collective-permute-start.1 = (bf16[512,2,128]{2,0,1:T(8,128)(2,1)S(1)}, bf16[512,2,128]{2,0,1:T(8,128)(2,1)S(1)}, u32[]{:S(2)}, u32[]{:S(2)}) collective-permute-start(bf16[512,2,128]{2,0,1:T(8,128)(2,1)S(1)} %collective-permute-done), channel_id=1, source_target_pairs={{0,4},{4,8},{8,12},{12,16},{16,20},{20,24},{24,28},{28,0},{1,5},{5... | collective-permute-start | bytes 786440 | tf_op jit(solution)/shard_map/ppermute | solution.py:120
  39.8 14.0 %collective-permute-start.2 = (bf16[512,2,128]{2,0,1:T(8,128)(2,1)S(1)}, bf16[512,2,128]{2,0,1:T(8,128)(2,1)S(1)}, u32[]{:S(2)}, u32[]{:S(2)}) collective-permute-start(bf16[512,2,128]{2,0,1:T(8,128)(2,1)S(1)} %collective-permute-done.1), channel_id=1, source_target_pairs={{0,4},{4,8},{8,12},{12,16},{16,20},{20,24},{24,28},{28,0},{1,5},{5... | collective-permute-start | bytes 786440 | tf_op jit(solution)/shard_map/ppermute | solution.py:120
  53.8 12.7 %collective-permute-start.3 = (bf16[512,2,128]{2,0,1:T(8,128)(2,1)S(1)}, bf16[512,2,128]{2,0,1:T(8,128)(2,1)S(1)}, u32[]{:S(2)}, u32[]{:S(2)}) collective-permute-start(bf16[512,2,128]{2,0,1:T(8,128)(2,1)S(1)} %collective-permute-done.2), channel_id=1, source_target_pairs={{0,4},{4,8},{8,12},{12,16},{16,20},{20,24},{24,28},{28,0},{1,5},{5... | collective-permute-start | bytes 786440 | tf_op jit(solution)/shard_map/ppermute | solution.py:120
  54.4 20.8 %collective-permute-start.10 = (bf16[256,2,256]{0,2,1:T(8,128)(2,1)S(1)}, bf16[256,2,256]{0,2,1:T(8,128)(2,1)S(1)}, u32[]{:S(2)}, u32[]{:S(2)}) collective-permute-start(bf16[256,2,256]{0,2,1:T(8,128)(2,1)S(1)} %copy.86), channel_id=1, source_target_pairs={{0,4},{4,0},{8,12},{12,8},{16,20},{20,16},{24,28},{28,24},{1,5},{5... | collective-permute-start | bytes 786440 | tf_op jit(solution)/shard_map/ppermute | solution.py:16
  66.5 13.3 %collective-permute-start.4 = (bf16[512,2,128]{2,0,1:T(8,128)(2,1)S(1)}, bf16[512,2,128]{2,0,1:T(8,128)(2,1)S(1)}, u32[]{:S(2)}, u32[]{:S(2)}) collective-permute-start(bf16[512,2,128]{2,0,1:T(8,128)(2,1)S(1)} %collective-permute-done.3), channel_id=1, source_target_pairs={{0,4},{4,8},{8,12},{12,16},{16,20},{20,24},{24,28},{28,0},{1,5},{5... | collective-permute-start | bytes 786440 | tf_op jit(solution)/shard_map/ppermute | solution.py:120
  75.1 12.4 %collective-permute-start.11 = (bf16[256,2,256]{0,2,1:T(8,128)(2,1)S(1)}, bf16[256,2,256]{0,2,1:T(8,128)(2,1)}, u32[]{:S(2)}, u32[]{:S(2)}) collective-permute-start(bf16[256,2,256]{0,2,1:T(8,128)(2,1)S(1)} %collective-permute-done.10), channel_id=1, source_target_pairs={{0,8},{4,12},{8,0},{12,4},{16,24},{20,28},{24,16},{28,20},{1,9},{5... | collective-permute-start | bytes 786440 | tf_op jit(solution)/shard_map/ppermute | solution.py:16
  79.8 12.1 %collective-permute-start.5 = (bf16[512,2,128]{2,0,1:T(8,128)(2,1)S(1)}, bf16[512,2,128]{2,0,1:T(8,128)(2,1)}, u32[]{:S(2)}, u32[]{:S(2)}) collective-permute-start(bf16[512,2,128]{2,0,1:T(8,128)(2,1)S(1)} %collective-permute-done.4), channel_id=1, source_target_pairs={{0,4},{4,8},{8,12},{12,16},{16,20},{20,24},{24,28},{28,0},{1,5},{5... | collective-permute-start | bytes 786440 | tf_op jit(solution)/shard_map/ppermute | solution.py:120
  80.0 7.5 collective-permute-start.7
  87.5 6.8 collective-permute-start.8
  87.5 27.3 %collective-permute-start.12 = (bf16[256,2,256]{0,2,1:T(8,128)(2,1)}, bf16[256,2,256]{0,2,1:T(8,128)(2,1)S(1)}, u32[]{:S(2)}, u32[]{:S(2)}) collective-permute-start(bf16[256,2,256]{0,2,1:T(8,128)(2,1)} %collective-permute-done.11), channel_id=1, source_target_pairs={{0,16},{4,20},{8,24},{12,28},{16,0},{20,4},{24,8},{28,12},{1,17},{... | collective-permute-start | bytes 786440 | tf_op jit(solution)/shard_map/ppermute | solution.py:16
  91.9 24.8 %collective-permute-start.6 = (bf16[512,2,128]{2,0,1:T(8,128)(2,1)}, bf16[512,2,128]{2,0,1:T(8,128)(2,1)}, u32[]{:S(2)}, u32[]{:S(2)}) collective-permute-start(bf16[512,2,128]{2,0,1:T(8,128)(2,1)} %collective-permute-done.5), channel_id=1, source_target_pairs={{0,4},{4,8},{8,12},{12,16},{16,20},{20,24},{24,28},{28,0},{1,5},{5... | collective-permute-start | bytes 786440 | tf_op jit(solution)/shard_map/ppermute | solution.py:120
  94.3 20.4 %collective-permute-start.9 = (bf16[256,2,128]{2,1,0:T(2,128)(2,1)S(1)}, bf16[256,2,128]{2,1,0:T(2,128)(2,1)S(1)}, u32[]{:S(2)}, u32[]{:S(2)}) collective-permute-start(bf16[256,2,128]{2,1,0:T(2,128)(2,1)S(1)} %collective-permute-done.8), channel_id=1, source_target_pairs={{0,16},{4,20},{8,24},{12,28},{16,0},{20,4},{24,8},{28,12},{1,17},{... | collective-permute-start | bytes 393224 | tf_op jit(solution)/shard_map/ppermute | solution.py:16
  95.0 339.3 %all-reduce.2.cloned.1.call-start = ((), (), s32[]{:S(2)}) async-start(), calls=%async_computation.5 | async-start | bytes 4194304 | tf_op jit(solution)/shard_map/psum | solution.py:168
  371.1 7.7 %collective-permute-start.18 = (bf16[256,256]{0,1:T(8,128)(2,1)S(1)}, bf16[256,256]{0,1:T(8,128)(2,1)S(1)}, u32[]{:S(2)}, u32[]{:S(2)}) collective-permute-start(bf16[256,256]{0,1:T(8,128)(2,1)S(1)} %collective-permute-done.17), channel_id=1, source_target_pairs={{0,16},{4,20},{8,24},{12,28},{16,0},{20,4},{24,8},{28,12},{1,17},{... | collective-permute-start | bytes 393224 | tf_op jit(solution)/shard_map/ppermute | solution.py:16
  373.4 8.2 %collective-permute-start.15 = (bf16[256,256]{0,1:T(8,128)(2,1)S(1)}, bf16[256,256]{0,1:T(8,128)(2,1)S(1)}, u32[]{:S(2)}, u32[]{:S(2)}) collective-permute-start(bf16[256,256]{0,1:T(8,128)(2,1)S(1)} %collective-permute-done.14), channel_id=1, source_target_pairs={{0,16},{4,20},{8,24},{12,28},{16,0},{20,4},{24,8},{28,12},{1,17},{... | collective-permute-start | bytes 393224 | tf_op jit(solution)/shard_map/ppermute | solution.py:16
  383.7 145.1 %all-gather.16.cloned.1.call-start = ((), (), s32[]{:S(2)}) async-start(), calls=%async_computation.6 | async-start | bytes 6488064 | tf_op jit(solution)/shard_map/all_gather | solution.py:181
  384.3 237.2 %all-gather.18.cloned.1.call-start = ((), (), s32[]{:S(2)}) async-start(), calls=%async_computation.7 | async-start | bytes 6488064 | tf_op jit(solution)/shard_map/all_gather | solution.py:186
  385.0 329.8 %all-gather.20.cloned.1.call-start = ((), (), s32[]{:S(2)}) async-start(), calls=%async_computation.8 | async-start | bytes 6488064 | tf_op jit(solution)/shard_map/all_gather | solution.py:189
  385.8 371.8 %reduce-scatter.2.cloned.1.call-start = ((), (), s32[]{:S(2)}) async-start(), calls=%async_computation.9 | async-start | bytes 2621440 | tf_op jit(solution)/shard_map/reduce_scatter | solution.py:191
  (57 other events, 911.0 us)
Sparse Core Ops, SparseCore 0:
  9.5 76.7 all-gather.9
  88.4 83.5 all-gather.13
  174.2 47.5 all-gather.11
  223.2 21.0 all-gather.7
  383.8 50.4 all-reduce.1
  436.4 92.3 all-gather.15
  530.9 90.4 all-gather.17
  623.5 91.2 all-gather.19
  728.2 29.3 reduce-scatter.1
